TPU v7x, 32 devices: a whole 2x2x4 slice. The times are simulated.
32 devices in a mesh: sp: 8 (over z, y), tp: 4 (over x, core).
Axes of the slice: x: 2, y: 2, z: 4, core: 2. Of those that a mesh axis runs over, the one named last changes fastest.
Arguments:
- stream: bfloat16 [2048, 2048], P('sp', 'tp'), may hold values from -1200 to 1200, as said below
- mix_gain: bfloat16 [2048], P('tp'), may hold values from 0.099609375 to 1.8984375
- pool_weight: bfloat16 [4, 512, 512], P('tp'), may hold values from -0.25 to 0.25
- pool_scale: bfloat16 [2048], P('tp'), may hold values from 0.099609375 to 1.8984375
- ffn_gain: bfloat16 [2048], replicated, may hold values from 0.099609375 to 1.8984375
- routes: int32 [2048, 2], P(('sp', 'tp')), may hold values from 0 to 7, all different within a row; in each aligned block of 64 rows (0 to 63, 64 to 127, ...) at most 32 rows name the same one
- route_weight: float32 [2048, 2], P(('sp', 'tp')), may hold values from 0.1 to 1
- w_gate: bfloat16 [8, 2048, 7168], P('sp', None, 'tp'), may hold values from -0.125 to 0.125
- w_up: bfloat16 [8, 2048, 7168], P('sp', None, 'tp'), may hold values from -0.125 to 0.125
- w_down: bfloat16 [8, 7168, 2048], P('sp', 'tp'), may hold values from -0.0625 to 0.0625
Outputs:
- layer_out: bfloat16 [2048, 2048], P(('sp', 'tp'))
Inputs may be any that keep to these rules, and one draw needn't show every extreme that they name: `routes`: each row names 2 different experts. Within each aligned block of 64 rows (the rows of one device) no expert is named by more than 32 rows, a bound that some block reaches. `stream`: finite values.
All inputs are finite; a program needn't handle non-finite values.
Results may differ from a plain program's by a relative error of at most 0.0061.
Values may be sent and summed in bfloat16 or wider, within the bound.
A program may use at most 128 MiB of HBM per device.

v0:
```python
import functools

import jax
import jax.numpy as jnp
from jax import lax
from jax.experimental import pallas as pl
from jax.experimental.pallas import tpu as pltpu
from jax.sharding import PartitionSpec as P

NORM_EPS = 1e-06


MESH = pl.DeviceIdType.MESH
COL_TILE = 256
LANES = 2
CHUNK_UNITS = (2, 2, 2, 1, 1)
PLAN = {
    "pre": "s0 p0 s1 e0",
    "0l": "p1 s2",
    "0z": "e1",
    "1e": "a0 s3",
    "1l": "p2 s4",
    "1z": "e2",
    "2e": "a1 b0",
    "2l": "p3 p4",
    "2z": "e3",
    "3e": "a2 b1",
    "3z": "e4",
    "4e": "a3 b2",
    "post": "a4 b3 b4",
}
SINGLE_PLAN = {"pre": "s0 p0 e0", "post": "a0 b0"}


def as_rows(block):
    width = block.shape[-1]
    if block.shape[-2] % 16:
        return block.astype(jnp.float32).reshape(-1, width).astype(block.dtype)
    return block.reshape(-1, width)


def moves(sp_count):
    far = [(pairs, inner) for pairs in range(1, sp_count // LANES) for inner in range(LANES)]
    return [(0, 0), (0, 1)] + far


def slot_of(expert, me, sp_count):
    pairs = (expert >> 1) - me // LANES
    pairs = jnp.where(pairs < 0, pairs + sp_count // LANES, pairs)
    inner = jnp.where((expert & 1) == lax.rem(me, LANES), 0, 1)
    return pairs * LANES + inner


def as_column(row):
    size = row.shape[1]
    rows = lax.broadcasted_iota(jnp.int32, (size, size), 0)
    columns = lax.broadcasted_iota(jnp.int32, (size, size), 1)
    return jnp.sum(jnp.where(rows == columns, row, 0.0), axis=1, keepdims=True)


def as_row(column):
    size = column.shape[0]
    rows = lax.broadcasted_iota(jnp.int32, (size, size), 0)
    columns = lax.broadcasted_iota(jnp.int32, (size, size), 1)
    return jnp.sum(jnp.where(rows == columns, column, 0.0), axis=0, keepdims=True)


def moved(me, move, sp_count):
    pairs_count = sp_count // LANES
    pairs = lax.rem(me // LANES + move[0], pairs_count)
    return pairs * LANES + lax.rem(me + move[1], LANES)


def moved_back(me, move, sp_count):
    pairs_count = sp_count // LANES
    pairs = lax.rem(me // LANES - move[0] + pairs_count, pairs_count)
    return pairs * LANES + lax.rem(me + move[1], LANES)


def chunk_sizes(sp_count):
    if sp_count % 8:
        return [sp_count]
    return [unit * (sp_count // 8) for unit in CHUNK_UNITS]


def col_tile(width):
    return COL_TILE if width % COL_TILE == 0 else width


def expert_kernel(
    sp_count,
    tp_count,
    cap,
    stream_ref,
    mix_ref,
    pool_ref,
    scale_ref,
    gain_ref,
    routes_ref,
    weight_ref,
    gate_hbm,
    up_hbm,
    down_hbm,
    out_ref,
    squares,
    tail,
    halo,
    mixed,
    tokens,
    picked_at,
    send_ref,
    gate,
    up,
    down,
    arrived,
    hidden,
    partial,
    pair_in,
    pair_sum,
    side_in,
    served,
    returned,
    square_sem,
    halo_sem,
    token_sem,
    local_sem,
    first_send,
    first_recv,
    side_send,
    side_recv,
    pair_send,
    pair_recv,
    back_pair,
    back_side,
    back_send,
    back_recv,
):
    me = lax.axis_index("sp")
    tp_me = lax.axis_index("tp")
    high, low = tp_me // LANES, lax.rem(tp_me, LANES)
    highs = tp_count // LANES
    other_low = 1 - low
    pair_id = {"sp": me, "tp": high * LANES + other_low}
    route = moves(sp_count)
    sizes = chunk_sizes(sp_count)
    chunks = len(sizes)
    starts = [sum(sizes[:index]) for index in range(chunks)]
    width = send_ref.shape[2]
    ff_width = gate.shape[1]
    half_width = width // 2

    def side_high(distance):
        return lax.rem(high + distance, highs)

    def side_id(distance):
        return {"sp": me, "tp": side_high(distance) * LANES + low}

    def from_high(distance):
        return lax.rem(high - distance + highs, highs)

    def tp_id(distance):
        return {"sp": me, "tp": lax.rem(tp_me + distance, tp_count)}

    def from_tp(distance):
        return lax.rem(tp_me - distance + tp_count, tp_count)

    weight_copies = [
        pltpu.make_async_copy(source.at[0], target, local_sem.at[index])
        for index, (source, target) in enumerate(((gate_hbm, gate), (up_hbm, up), (down_hbm, down)))
    ]
    own_copy = pltpu.make_async_copy(send_ref.at[0], arrived.at[0, low, high], local_sem.at[3])
    for copy in weight_copies:
        copy.start()

    barrier = pltpu.get_barrier_semaphore()
    for step in range(1, sp_count):
        pl.semaphore_signal(
            barrier,
            inc=1,
            device_id={"sp": moved(me, route[step], sp_count), "tp": tp_me},
            device_id_type=MESH,
        )
    for distance in range(1, tp_count):
        pl.semaphore_signal(barrier, inc=1, device_id=tp_id(distance), device_id_type=MESH)

    def square_copy(distance):
        return pltpu.make_async_remote_copy(
            src_ref=squares.at[0],
            dst_ref=squares.at[distance],
            send_sem=square_sem.at[0, distance - 1],
            recv_sem=square_sem.at[1, distance - 1],
            device_id=tp_id(distance),
            device_id_type=MESH,
        )

    halo_copy = pltpu.make_async_remote_copy(
        src_ref=tail,
        dst_ref=halo,
        send_sem=halo_sem.at[0],
        recv_sem=halo_sem.at[1],
        device_id={"sp": lax.rem(me + 1, sp_count), "tp": tp_me},
        device_id_type=MESH,
    )

    def token_copy(distance):
        return pltpu.make_async_remote_copy(
            src_ref=mixed.at[lax.rem(tp_me + distance, tp_count)],
            dst_ref=tokens.at[tp_me],
            send_sem=token_sem.at[0, distance - 1],
            recv_sem=token_sem.at[1, distance - 1],
            device_id=tp_id(distance),
            device_id_type=MESH,
        )

    tok_rows, group_width = stream_ref.shape
    halo_rows = halo.shape[0]
    tok_count = tokens.shape[1]
    top_count = routes_ref.shape[0]
    slot_count = sp_count * cap
    stream_f32 = stream_ref[...].astype(jnp.float32)
    own_square = as_row(jnp.sum(stream_f32 * stream_f32, axis=1, keepdims=True))
    squares[0] = jnp.broadcast_to(own_square, squares.shape[1:])
    pl.semaphore_wait(barrier, sp_count - 1 + tp_count - 1)
    for distance in range(1, tp_count):
        square_copy(distance).start()

    experts = lax.broadcasted_iota(jnp.int32, (128, tok_count), 0)
    named = [experts == routes_ref[pick : pick + 1, :] for pick in range(top_count)]
    hits = named[0].astype(jnp.float32)
    for pick in range(1, top_count):
        hits = hits + named[pick].astype(jnp.float32)
    earlier = lax.broadcasted_iota(jnp.int32, (tok_count, tok_count), 0)
    later = lax.broadcasted_iota(jnp.int32, (tok_count, tok_count), 1)
    before = jnp.where(earlier < later, 1.0, 0.0).astype(jnp.bfloat16)
    rank = jnp.dot(hits.astype(jnp.bfloat16), before, preferred_element_type=jnp.float32)
    slots = lax.broadcasted_iota(jnp.int32, (slot_count, tok_count), 0).astype(jnp.float32)
    picks = []
    for pick in range(top_count):
        start = slot_of(routes_ref[pick : pick + 1, :], me, sp_count) * cap
        spot = jnp.sum(jnp.where(named[pick], rank, 0.0), axis=0, keepdims=True)
        spot = spot + start.astype(jnp.float32)
        picks.append(jnp.where(slots == spot, 1.0, 0.0))
    dispatch = sum(picks[1:], picks[0]).astype(jnp.bfloat16)
    for pick in range(top_count):
        picked_at[pick] = picks[pick].astype(jnp.bfloat16)

    window_len = jnp.left_shift(jnp.int32(2), tp_me)
    first_row = me * tok_rows
    row_at = lax.broadcasted_iota(jnp.int32, (tok_rows, tok_rows), 0)
    source_at = lax.broadcasted_iota(jnp.int32, (tok_rows, tok_rows), 1)
    lag = row_at - source_at
    band = jnp.where((lag >= 0) & (lag < window_len), 1.0, 0.0).astype(jnp.bfloat16)
    row_at = lax.broadcasted_iota(jnp.int32, (tok_rows, halo_rows), 0)
    source_at = lax.broadcasted_iota(jnp.int32, (tok_rows, halo_rows), 1) - halo_rows
    reach = (row_at - source_at < window_len) & (first_row + source_at >= 0)
    halo_band = jnp.where(reach, 1.0, 0.0).astype(jnp.bfloat16)
    position = first_row + lax.broadcasted_iota(jnp.int32, (tok_rows, 1), 0)
    window_count = jnp.minimum(position + 1, window_len).astype(jnp.float32)

    for distance in range(1, tp_count):
        square_copy(distance).wait_recv()
    square = squares[0, 0:1, :]
    for distance in range(1, tp_count):
        square = square + squares[distance, 0:1, :]
    row_scale = lax.rsqrt(as_column(square) / width + NORM_EPS)
    normed = stream_f32 * row_scale * mix_ref[...].astype(jnp.float32)[None, :]
    normed = normed.astype(jnp.bfloat16)
    tail[...] = normed[tok_rows - halo_rows :]
    halo_copy.start()
    window_sum = jnp.dot(band, normed, preferred_element_type=jnp.float32)
    halo_copy.wait_recv()
    window_sum = window_sum + jnp.dot(halo_band, halo[...], preferred_element_type=jnp.float32)
    pooled = (window_sum / window_count - normed.astype(jnp.float32)).astype(jnp.bfloat16)
    mixer_out = jnp.dot(pooled, pool_ref[0], preferred_element_type=jnp.float32)
    mixer_out = mixer_out * scale_ref[...].astype(jnp.float32)[None, :]
    after_mix = (stream_f32 + mixer_out).astype(jnp.bfloat16)
    mixed[...] = after_mix.reshape(mixed.shape)
    for distance in range(1, tp_count):
        token_copy(distance).start()
    tokens[tp_me] = mixed[tp_me]
    for distance in range(1, tp_count):
        token_copy(distance).wait_recv()
    mean_square = jnp.zeros((tok_count, 1), jnp.float32)
    for piece in range(tp_count):
        after_f32 = tokens[piece].astype(jnp.float32)
        mean_square = mean_square + jnp.sum(after_f32 * after_f32, axis=1, keepdims=True)
    ffn_scale = lax.rsqrt(mean_square / width + NORM_EPS)
    for piece in range(tp_count):
        columns = slice(piece * group_width, (piece + 1) * group_width)
        gain = gain_ref[columns].astype(jnp.float32)[None, :]
        normed2 = (tokens[piece].astype(jnp.float32) * ffn_scale * gain).astype(jnp.bfloat16)
        rows = jnp.dot(dispatch, normed2, preferred_element_type=jnp.float32)
        rows = rows.reshape(sp_count, cap, group_width).astype(jnp.bfloat16)
        send_ref[:, :, columns] = rows

    def first_copy(step):
        return pltpu.make_async_remote_copy(
            src_ref=send_ref.at[step],
            dst_ref=arrived.at[step, low, high],
            send_sem=first_send.at[step],
            recv_sem=first_recv.at[step],
            device_id={"sp": moved(me, route[step], sp_count), "tp": tp_me},
            device_id_type=MESH,
        )

    def side_copy(step, distance):
        return pltpu.make_async_remote_copy(
            src_ref=arrived.at[step, low, high],
            dst_ref=arrived.at[step, low, high],
            send_sem=side_send.at[step, distance - 1],
            recv_sem=side_recv.at[step, distance - 1],
            device_id=side_id(distance),
            device_id_type=MESH,
        )

    def pair_copy(step, distance):
        block = arrived.at[step, low, from_high(distance)]
        return pltpu.make_async_remote_copy(
            src_ref=block,
            dst_ref=block,
            send_sem=pair_send.at[step, distance],
            recv_sem=pair_recv.at[step, distance],
            device_id=pair_id,
            device_id_type=MESH,
        )

    def chunk_steps(chunk):
        return range(starts[chunk], starts[chunk] + sizes[chunk])

    def spread(chunk):
        for step in chunk_steps(chunk):
            if step == 0:
                own_copy.wait()
            else:
                first_copy(step).wait_recv()
            for distance in range(1, highs):
                side_copy(step, distance).start()
            pair_copy(step, 0).start()

    def pass_on(chunk):
        for step in chunk_steps(chunk):
            for distance in range(1, highs):
                side_copy(step, distance).wait_recv()
                pair_copy(step, distance).start()

    def settle(chunk):
        for step in chunk_steps(chunk):
            for distance in range(highs):
                pair_copy(step, distance).wait_recv()

    def span(chunk):
        return pl.ds(starts[chunk], sizes[chunk])

    def row_span(chunk):
        return pl.ds(0, sizes[chunk] * tp_count * cap)

    def gate_up(chunk, first, last):
        tile = col_tile(ff_width)

        def body(index, carry):
            columns = pl.ds(pl.multiple_of(index * tile, tile), tile)
            rows = as_rows(arrived[span(chunk)])
            gate_val = jnp.dot(rows, gate[:, columns], preferred_element_type=jnp.float32)
            up_val = jnp.dot(rows, up[:, columns], preferred_element_type=jnp.float32)
            hidden[row_span(chunk), columns] = (jax.nn.silu(gate_val) * up_val).astype(jnp.bfloat16)
            return carry

        lax.fori_loop(first, last, body, 0)

    def project(chunk, half):
        tile = col_tile(half_width)
        first = half * half_width // tile

        def body(index, carry):
            columns = pl.ds(pl.multiple_of(index * tile, tile), tile)
            block = jnp.dot(
                hidden[row_span(chunk), :], down[:, columns], preferred_element_type=jnp.float32
            )
            block = block.reshape(sizes[chunk], LANES, highs, cap, tile).astype(jnp.bfloat16)
            partial[span(chunk), :, :, :, columns] = block
            return carry

        lax.fori_loop(first, first + half_width // tile, body, 0)

    def part(half):
        return pl.ds(half * half_width, half_width)

    def back_pair_copy(chunk, half):
        return pltpu.make_async_remote_copy(
            src_ref=partial.at[span(chunk), other_low, :, :, part(half)],
            dst_ref=pair_in.at[span(chunk), :, :, part(half)],
            send_sem=back_pair.at[0, chunk, half],
            recv_sem=back_pair.at[1, chunk, half],
            device_id=pair_id,
            device_id_type=MESH,
        )

    def back_side_copy(chunk, half, distance):
        return pltpu.make_async_remote_copy(
            src_ref=pair_sum.at[distance - 1, span(chunk), :, part(half)],
            dst_ref=side_in.at[distance - 1, span(chunk), :, part(half)],
            send_sem=back_side.at[0, chunk, half, distance - 1],
            recv_sem=back_side.at[1, chunk, half, distance - 1],
            device_id=side_id(distance),
            device_id_type=MESH,
        )

    def back_copy(step, half):
        return pltpu.make_async_remote_copy(
            src_ref=served.at[step, :, part(half)],
            dst_ref=returned.at[step, :, part(half)],
            send_sem=back_send.at[step, half],
            recv_sem=back_recv.at[step, half],
            device_id={"sp": moved_back(me, route[step], sp_count), "tp": tp_me},
            device_id_type=MESH,
        )

    def pair_add(chunk, half):
        back_pair_copy(chunk, half).wait_recv()
        for distance in range(1, highs):
            target = side_high(distance)

            def body(index, carry, distance=distance, target=target):
                step = starts[chunk] + index
                total = partial[step, low, target, :, part(half)].astype(jnp.float32)
                total = total + pair_in[step, target, :, part(half)].astype(jnp.float32)
                pair_sum[distance - 1, step, :, part(half)] = total.astype(jnp.bfloat16)
                return carry

            lax.fori_loop(0, sizes[chunk], body, 0)
            back_side_copy(chunk, half, distance).start()

    def side_add(chunk, half):
        for distance in range(1, highs):
            back_side_copy(chunk, half, distance).wait_recv()
        for step in chunk_steps(chunk):
            total = partial[step, low, high, :, part(half)].astype(jnp.float32)
            total = total + pair_in[step, high, :, part(half)].astype(jnp.float32)
            for distance in range(1, highs):
                total = total + side_in[distance - 1, step, :, part(half)].astype(jnp.float32)
            if step == 0:
                returned[0, :, part(half)] = total.astype(jnp.bfloat16)
            else:
                served[step, :, part(half)] = total.astype(jnp.bfloat16)
                back_copy(step, half).start()

    own_copy.start()
    for step in range(1, sp_count):
        first_copy(step).start()

    plan = PLAN if chunks == len(CHUNK_UNITS) else SINGLE_PLAN
    acts = {"s": spread, "p": pass_on, "e": settle}
    adds = {"a": pair_add, "b": side_add}

    def run(place):
        for name in plan.get(place, "").split():
            if name[0] in acts:
                acts[name[0]](int(name[1]))
            elif len(name) > 2:
                adds[name[0]](int(name[1]), int(name[2]))
            else:
                for half in range(2):
                    adds[name[0]](int(name[1]), half)

    run("pre")
    for copy in weight_copies:
        copy.wait()
    tiles = ff_width // col_tile(ff_width)
    early, late = tiles // 2, tiles - tiles // 4
    for chunk in range(chunks):
        gate_up(chunk, 0, early)
        run(f"{chunk}e")
        gate_up(chunk, early, late)
        run(f"{chunk}m")
        gate_up(chunk, late, tiles)
        run(f"{chunk}l")
        for half in range(2):
            project(chunk, half)
            back_pair_copy(chunk, half).start()
            run(f"{chunk}h" if half == 0 else f"{chunk}z")
    run("post")

    for step in range(1, sp_count):
        for half in range(2):
            back_copy(step, half).wait_recv()
    rows = as_rows(returned[...])
    route_weights = [as_column(weight_ref[pick : pick + 1, :]) for pick in range(top_count)]
    for piece in range(tp_count):
        columns = slice(piece * group_width, (piece + 1) * group_width)
        total = tokens[piece].astype(jnp.float32)
        for pick in range(top_count):
            picked = lax.dot_general(
                picked_at[pick],
                rows[:, columns],
                (((0,), (0,)), ((), ())),
                preferred_element_type=jnp.float32,
            )
            total = total + route_weights[pick] * picked
        out_ref[:, columns] = total.astype(jnp.bfloat16)

    halo_copy.wait_send()
    for distance in range(1, tp_count):
        square_copy(distance).wait_send()
        token_copy(distance).wait_send()
    for step in range(sp_count):
        if step > 0:
            first_copy(step).wait_send()
            for half in range(2):
                back_copy(step, half).wait_send()
        for distance in range(1, highs):
            side_copy(step, distance).wait_send()
        for distance in range(highs):
            pair_copy(step, distance).wait_send()
    for chunk in range(chunks):
        for half in range(2):
            back_pair_copy(chunk, half).wait_send()
            for distance in range(1, highs):
                back_side_copy(chunk, half, distance).wait_send()


def per_device(
    stream, mix_gain, pool_weight, pool_scale, ffn_gain, routes, route_weight, w_gate, w_up, w_down
):
    tok_rows, group_width = stream.shape
    tp_count = lax.axis_size("tp")
    sp_count = lax.axis_size("sp")
    width = group_width * tp_count
    tok_count, top_count = routes.shape
    cap = 2 * tok_count * top_count // sp_count
    halo_rows = 2 ** (pool_weight.shape[0] * tp_count)
    highs = tp_count // LANES
    chunks = len(chunk_sizes(sp_count))
    chunk_rows = max(chunk_sizes(sp_count)) * tp_count * cap
    ff_width = w_gate.shape[2]
    half = jnp.bfloat16
    vmem = pl.BlockSpec(memory_space=pltpu.VMEM)
    hbm = pl.BlockSpec(memory_space=pl.ANY)
    dma = pltpu.SemaphoreType.DMA
    return pl.pallas_call(
        functools.partial(expert_kernel, sp_count, tp_count, cap),
        out_shape=jax.ShapeDtypeStruct((tok_count, width), half),
        in_specs=[vmem] * 7 + [hbm] * 3,
        out_specs=vmem,
        scratch_shapes=[
            pltpu.VMEM((tp_count, 8, tok_rows), jnp.float32),
            pltpu.VMEM((halo_rows, group_width), half),
            pltpu.VMEM((halo_rows, group_width), half),
            pltpu.VMEM((tp_count, tok_count, group_width), half),
            pltpu.VMEM((tp_count, tok_count, group_width), half),
            pltpu.VMEM((top_count, sp_count * cap, tok_count), half),
            pltpu.VMEM((sp_count, cap, width), half),
            pltpu.VMEM(w_gate.shape[1:], half),
            pltpu.VMEM(w_up.shape[1:], half),
            pltpu.VMEM(w_down.shape[1:], half),
            pltpu.VMEM((sp_count, LANES, highs, cap, width), half),
            pltpu.VMEM((chunk_rows, ff_width), half),
            pltpu.VMEM((sp_count, LANES, highs, cap, width), half),
            pltpu.VMEM((sp_count, highs, cap, width), half),
            pltpu.VMEM((highs - 1, sp_count, cap, width), half),
            pltpu.VMEM((highs - 1, sp_count, cap, width), half),
            pltpu.VMEM((sp_count, cap, width), half),
            pltpu.VMEM((sp_count, cap, width), half),
            dma((2, tp_count - 1)),
            dma((2,)),
            dma((2, tp_count - 1)),
            dma((4,)),
            dma((sp_count,)),
            dma((sp_count,)),
            dma((sp_count, highs - 1)),
            dma((sp_count, highs - 1)),
            dma((sp_count, highs)),
            dma((sp_count, highs)),
            dma((2, chunks, 2)),
            dma((2, chunks, 2, highs - 1)),
            dma((sp_count, 2)),
            dma((sp_count, 2)),
        ],
        compiler_params=pltpu.CompilerParams(
            collective_id=1, has_side_effects=True, vmem_limit_bytes=60 * 1024 * 1024
        ),
    )(
        stream,
        mix_gain,
        pool_weight,
        pool_scale,
        ffn_gain,
        routes.T,
        route_weight.T,
        w_gate,
        w_up,
        w_down,
    )


def solution(mesh):
    in_specs = (
        P("sp", "tp"),
        P("tp"),
        P("tp", None, None),
        P("tp"),
        P(),
        P(("sp", "tp"), None),
        P(("sp", "tp"), None),
        P("sp", None, "tp"),
        P("sp", None, "tp"),
        P("sp", "tp", None),
    )
    out_specs = P(("sp", "tp"), None)
    return jax.shard_map(
        per_device, mesh=mesh, in_specs=in_specs, out_specs=out_specs, check_vma=False
    )
```

profile of v0, /device:TPU:0, one launch (start us, length us, event | category | flops | bytes accessed | tf_op | source)
XLA Modules:
  0.0 95.7 jit_solution(14400592148855992235)
XLA Ops:
  0.0 94.0 %shard_map.100 = bf16[64,2048]{1,0:T(8,128)(2,1)} custom-call(bf16[256,512]{1,0:T(8,128)(2,1)} %stream_ref.1, bf16[512]{0:T(512)(128)(2,1)} %mix_ref.1, bf16[1,512,512]{2,1,0:T(8,128)(2,1)} %pool_ref.1, bf16[512]{0:T(512)(128)(2,1)} %scale_ref.1, bf16[2048]{0:T(1024)(128)(2,1)} %gain_ref.1, s32[2,64]{1,0:T(2,128)} %bitcast.2, f32[2,64]{1,0:T(2,128)} %bitcast.3, ...), custom_call_target="tpu_custom_call" | custom-call | tf_op jit(solution)/shard_map/pallas_call | solution.py:539
  94.0 1.7 %copy.12 = bf16[64,2048]{1,0:T(8,128)(2,1)} copy(bf16[64,2048]{1,0:T(8,128)(2,1)} %shard_map.100) | data formatting | bytes 524288
where the time goes:
time: 95.9 us; the launch traced here: 95.7 us
  Pallas kernels  94 us (98%)
  local copies, waits for them, and re-layouts  1.67 us (2%)
    pallas_call x1, Pallas kernels, per_device(): pl.pallas_call(functools.partial(expert_kernel, sp_count, tp_count, cap),...  94 us

commit v1 on v0

v1 whole, which is shorter than its diff:
```python
import functools

import jax
import jax.numpy as jnp
from jax import lax
from jax.experimental import pallas as pl
from jax.experimental.pallas import tpu as pltpu
from jax.sharding import PartitionSpec as P

NORM_EPS = 1e-06


MESH = pl.DeviceIdType.MESH
COL_TILE = 256
LANES = 2
CHUNKS = 8
SPREAD_AHEAD = 3
PASS_AHEAD = 1
SIDE_LAG = 2


def as_rows(block):
    width = block.shape[-1]
    if block.shape[-2] % 16:
        return block.astype(jnp.float32).reshape(-1, width).astype(block.dtype)
    return block.reshape(-1, width)


def flip(code, sp_count):
    return jnp.where(code == 0, 0, sp_count - code)


def turned(me, code, sp_count):
    if sp_count != 4 * LANES:
        return code
    inside = ((me // LANES == 1) | (me // LANES == 2)) & (code >= sp_count // 2)
    return jnp.where(inside, code ^ LANES, code)


def step_of(peer, me, sp_count):
    return flip(turned(me, peer ^ me, sp_count), sp_count)


def peer_of(step, me, sp_count):
    return turned(me, flip(step, sp_count), sp_count) ^ me


def as_column(row):
    size = row.shape[1]
    rows = lax.broadcasted_iota(jnp.int32, (size, size), 0)
    columns = lax.broadcasted_iota(jnp.int32, (size, size), 1)
    return jnp.sum(jnp.where(rows == columns, row, 0.0), axis=1, keepdims=True)


def as_row(column):
    size = column.shape[0]
    rows = lax.broadcasted_iota(jnp.int32, (size, size), 0)
    columns = lax.broadcasted_iota(jnp.int32, (size, size), 1)
    return jnp.sum(jnp.where(rows == columns, column, 0.0), axis=0, keepdims=True)


def chunk_count(sp_count):
    return CHUNKS if sp_count % CHUNKS == 0 else sp_count


def col_tile(width):
    return COL_TILE if width % COL_TILE == 0 else width


def expert_kernel(
    sp_count,
    tp_count,
    cap,
    stream_ref,
    mix_ref,
    pool_ref,
    scale_ref,
    gain_ref,
    routes_ref,
    weight_ref,
    gate_hbm,
    up_hbm,
    down_hbm,
    out_ref,
    squares,
    squares2,
    routes_all,
    tail,
    halo,
    mixed,
    tokens,
    picked_at,
    send_ref,
    gate,
    up,
    down,
    arrived,
    hidden,
    partial,
    pair_in,
    pair_sum,
    side_in,
    served,
    returned,
    round_sem,
    square_sem,
    square2_sem,
    route_sem,
    halo_sem,
    token_sem,
    local_sem,
    first_send,
    first_recv,
    side_send,
    side_recv,
    pair_send,
    pair_recv,
    back_pair,
    back_side,
    back_send,
    back_recv,
):
    me = lax.axis_index("sp")
    tp_me = lax.axis_index("tp")
    high, low = tp_me // LANES, lax.rem(tp_me, LANES)
    highs = tp_count // LANES
    other_low = 1 - low
    pair_id = {"sp": me, "tp": high * LANES + other_low}
    pairs_count = sp_count // LANES
    chunks = chunk_count(sp_count)
    group = sp_count // chunks
    ff_width = gate.shape[1]
    tok_rows, group_width = stream_ref.shape
    width = group_width * tp_count
    halo_rows = halo.shape[0]
    tok_count = tokens.shape[1]
    top_count = routes_ref.shape[0]
    slot_count = sp_count * cap
    chunk_rows = hidden.shape[0]

    def side_high(distance):
        return lax.rem(high + distance, highs)

    def side_id(distance):
        return {"sp": me, "tp": side_high(distance) * LANES + low}

    def from_high(distance):
        return lax.rem(high - distance + highs, highs)

    def tp_id(distance):
        return {"sp": me, "tp": lax.rem(tp_me + distance, tp_count)}

    def sp_id(peer):
        return {"sp": peer, "tp": tp_me}

    def columns_of(piece):
        return pl.ds(pl.multiple_of(piece * group_width, group_width), group_width)

    weight_copies = [
        pltpu.make_async_copy(source.at[0], target, local_sem.at[index])
        for index, (source, target) in enumerate(((gate_hbm, gate), (up_hbm, up), (down_hbm, down)))
    ]
    for copy in weight_copies:
        copy.start()

    barrier = pltpu.get_barrier_semaphore()
    beside = me ^ 1
    across = jnp.where(lax.rem(me, LANES) == 1, me + 1, me - 1)
    has_across = (across >= 0) & (across < sp_count)
    has_up = me + LANES < sp_count
    has_down = me - LANES >= 0
    near_count = 1 + has_up.astype(jnp.int32) + has_down.astype(jnp.int32)

    def tell_near(sem):
        pl.semaphore_signal(sem, inc=1, device_id=sp_id(beside), device_id_type=MESH)

        @pl.when(has_up)
        def _():
            pl.semaphore_signal(sem, inc=1, device_id=sp_id(me + LANES), device_id_type=MESH)

        @pl.when(has_down)
        def _():
            pl.semaphore_signal(sem, inc=1, device_id=sp_id(me - LANES), device_id_type=MESH)

    for distance in range(1, tp_count):
        pl.semaphore_signal(barrier, inc=1, device_id=tp_id(distance), device_id_type=MESH)

    @pl.when(has_across)
    def _():
        pl.semaphore_signal(barrier, inc=1, device_id=sp_id(across), device_id_type=MESH)

    tell_near(barrier)

    def square_copy(distance):
        return pltpu.make_async_remote_copy(
            src_ref=squares.at[0],
            dst_ref=squares.at[distance],
            send_sem=square_sem.at[0, distance - 1],
            recv_sem=square_sem.at[1, distance - 1],
            device_id=tp_id(distance),
            device_id_type=MESH,
        )

    def square2_copy(distance):
        return pltpu.make_async_remote_copy(
            src_ref=squares2.at[0],
            dst_ref=squares2.at[distance],
            send_sem=square2_sem.at[0, distance - 1],
            recv_sem=square2_sem.at[1, distance - 1],
            device_id=tp_id(distance),
            device_id_type=MESH,
        )

    def route_copy(distance):
        return pltpu.make_async_remote_copy(
            src_ref=routes_ref,
            dst_ref=routes_all.at[tp_me],
            send_sem=route_sem.at[0, distance - 1],
            recv_sem=route_sem.at[1, distance - 1],
            device_id=tp_id(distance),
            device_id_type=MESH,
        )

    halo_copy = pltpu.make_async_remote_copy(
        src_ref=tail,
        dst_ref=halo,
        send_sem=halo_sem.at[0],
        recv_sem=halo_sem.at[1],
        device_id=sp_id(me + 1),
        device_id_type=MESH,
    )

    def token_copy(distance):
        return pltpu.make_async_remote_copy(
            src_ref=mixed.at[lax.rem(tp_me + distance, tp_count)],
            dst_ref=tokens.at[tp_me],
            send_sem=token_sem.at[0, distance - 1],
            recv_sem=token_sem.at[1, distance - 1],
            device_id=tp_id(distance),
            device_id_type=MESH,
        )

    stream_f32 = stream_ref[...].astype(jnp.float32)
    own_square = as_row(jnp.sum(stream_f32 * stream_f32, axis=1, keepdims=True))
    squares[0] = jnp.broadcast_to(own_square, squares.shape[1:])
    pl.semaphore_wait(barrier, tp_count - 1 + near_count + has_across.astype(jnp.int32))
    for distance in range(1, tp_count):
        square_copy(distance).start()
    for distance in range(1, tp_count):
        route_copy(distance).start()
    if pairs_count > 1:
        tell_near(round_sem.at[0])
    routes_all[tp_me] = routes_ref[...]

    window_len = jnp.left_shift(jnp.int32(2), tp_me)
    first_row = me * tok_rows
    row_at = lax.broadcasted_iota(jnp.int32, (tok_rows, tok_rows), 0)
    source_at = lax.broadcasted_iota(jnp.int32, (tok_rows, tok_rows), 1)
    lag = row_at - source_at
    band = jnp.where((lag >= 0) & (lag < window_len), 1.0, 0.0).astype(jnp.bfloat16)
    row_at = lax.broadcasted_iota(jnp.int32, (halo_rows, halo_rows), 0)
    source_at = lax.broadcasted_iota(jnp.int32, (halo_rows, halo_rows), 1) - halo_rows
    reach = (row_at - source_at < window_len) & (first_row + source_at >= 0)
    halo_band = jnp.where(reach, 1.0, 0.0).astype(jnp.bfloat16)
    position = first_row + lax.broadcasted_iota(jnp.int32, (tok_rows, 1), 0)
    window_count = jnp.minimum(position + 1, window_len).astype(jnp.float32)
    pool_scale = scale_ref[...].astype(jnp.float32)[None, :]

    for distance in range(1, tp_count):
        square_copy(distance).wait_recv()
    square = squares[0, 0:1, :]
    for distance in range(1, tp_count):
        square = square + squares[distance, 0:1, :]
    row_scale = lax.rsqrt(as_column(square) / width + NORM_EPS)
    normed = stream_f32 * row_scale * mix_ref[...].astype(jnp.float32)[None, :]
    normed = normed.astype(jnp.bfloat16)
    tail[...] = normed[tok_rows - halo_rows :]

    @pl.when(me + 1 < sp_count)
    def _():
        halo_copy.start()

    def mix(sums, counts, own, rows):
        pooled = (sums / counts - own.astype(jnp.float32)).astype(jnp.bfloat16)
        mixer_out = jnp.dot(pooled, pool_ref[0], preferred_element_type=jnp.float32)
        return (rows + mixer_out * pool_scale).astype(jnp.bfloat16)

    window_sum = jnp.dot(band, normed, preferred_element_type=jnp.float32)
    after_mix = mix(window_sum, window_count, normed, stream_f32)
    for piece in range(tp_count):
        mixed[piece] = after_mix[piece * tok_count : (piece + 1) * tok_count]

    def next_round(index):
        pl.semaphore_wait(round_sem.at[index], near_count)
        if index + 2 < pairs_count:
            tell_near(round_sem.at[index + 1])

    if pairs_count > 1:
        next_round(0)

    @pl.when(me > 0)
    def _():
        halo_copy.wait_recv()

    @pl.when(me == 0)
    def _():
        halo[...] = jnp.zeros_like(halo)

    first_sum = window_sum[:halo_rows]
    first_sum = first_sum + jnp.dot(halo_band, halo[...], preferred_element_type=jnp.float32)
    first_mix = mix(
        first_sum, window_count[:halo_rows], normed[:halo_rows], stream_f32[:halo_rows]
    )
    mixed[0, 0:halo_rows, :] = first_mix
    after_f32 = mixed[...].reshape(tok_rows, group_width).astype(jnp.float32)
    own_square = as_row(jnp.sum(after_f32 * after_f32, axis=1, keepdims=True))
    squares2[0] = jnp.broadcast_to(own_square, squares2.shape[1:])
    for distance in range(1, tp_count):
        square2_copy(distance).start()
    for distance in range(1, tp_count):
        token_copy(distance).start()
    tokens[tp_me] = mixed[tp_me]

    if pairs_count > 2:
        next_round(1)

    experts = lax.broadcasted_iota(jnp.int32, (128, tok_count), 0)
    earlier = lax.broadcasted_iota(jnp.int32, (tok_count, tok_count), 0)
    later = lax.broadcasted_iota(jnp.int32, (tok_count, tok_count), 1)
    before = jnp.where(earlier < later, 1.0, 0.0).astype(jnp.bfloat16)
    slots = lax.broadcasted_iota(jnp.int32, (slot_count, tok_count), 0).astype(jnp.float32)
    for distance in range(1, tp_count):
        route_copy(distance).wait_recv()
    for piece in range(tp_count):
        routes = routes_all[piece]
        named = [experts == routes[pick : pick + 1, :] for pick in range(top_count)]
        hits = named[0].astype(jnp.float32)
        for pick in range(1, top_count):
            hits = hits + named[pick].astype(jnp.float32)
        rank = jnp.dot(hits.astype(jnp.bfloat16), before, preferred_element_type=jnp.float32)
        for pick in range(top_count):
            start = step_of(routes[pick : pick + 1, :], me, sp_count) * cap
            spot = jnp.sum(jnp.where(named[pick], rank, 0.0), axis=0, keepdims=True)
            spot = spot + start.astype(jnp.float32)
            picked_at[piece, pick] = jnp.where(slots == spot, 1.0, 0.0).astype(jnp.bfloat16)
    gain = gain_ref[0:group_width]
    for piece in range(1, tp_count):
        columns = slice(piece * group_width, (piece + 1) * group_width)
        gain = jnp.where(tp_me == piece, gain_ref[columns], gain)
    gain = gain.astype(jnp.float32)[None, :]

    for distance in range(1, tp_count):
        square2_copy(distance).wait_recv()
    square = squares2[0, 0:1, :]
    for distance in range(1, tp_count):
        square = square + squares2[distance, 0:1, :]
    ffn_scale = lax.rsqrt(as_column(square) / width + NORM_EPS)
    normed2 = (after_f32 * ffn_scale * gain).astype(jnp.bfloat16)
    for index in range(2, pairs_count - 1):
        next_round(index)
    for piece in range(tp_count):
        dispatch = picked_at[piece, 0]
        for pick in range(1, top_count):
            dispatch = dispatch + picked_at[piece, pick]
        rows = jnp.dot(
            dispatch,
            normed2[piece * tok_count : (piece + 1) * tok_count],
            preferred_element_type=jnp.float32,
        )
        rows = rows.reshape(sp_count, cap, group_width).astype(jnp.bfloat16)
        send_ref[:, piece % LANES, piece // LANES] = rows

    def first_copy(step):
        peer = peer_of(step, me, sp_count)
        return pltpu.make_async_remote_copy(
            src_ref=send_ref.at[step],
            dst_ref=arrived.at[step_of(me, peer, sp_count), :, :, :, columns_of(tp_me)],
            send_sem=first_send.at[step],
            recv_sem=first_recv.at[step_of(me, peer, sp_count)],
            device_id=sp_id(peer),
            device_id_type=MESH,
        )

    def first_arrival(step):
        return pltpu.make_async_remote_copy(
            src_ref=send_ref.at[step],
            dst_ref=arrived.at[step, :, :, :, columns_of(tp_me)],
            send_sem=first_send.at[step],
            recv_sem=first_recv.at[step],
            device_id=sp_id(peer_of(step, me, sp_count)),
            device_id_type=MESH,
        )

    def side_copy(step, distance):
        block = arrived.at[step, :, :, :, columns_of(tp_me)]
        return pltpu.make_async_remote_copy(
            src_ref=block,
            dst_ref=block,
            send_sem=side_send.at[step, distance - 1],
            recv_sem=side_recv.at[step, distance - 1],
            device_id=side_id(distance),
            device_id_type=MESH,
        )

    def pair_copy(step, distance):
        piece = from_high(distance) * LANES + low
        block = arrived.at[step, :, :, :, columns_of(piece)]
        return pltpu.make_async_remote_copy(
            src_ref=block,
            dst_ref=block,
            send_sem=pair_send.at[step, distance],
            recv_sem=pair_recv.at[step, distance],
            device_id=pair_id,
            device_id_type=MESH,
        )

    def steps_of(chunk):
        return [chunk * group + index for index in range(group)]

    def share(step):
        for distance in range(1, highs):
            side_copy(step, distance).start()
        pair_copy(step, 0).start()

    def spread(chunk):
        for step in steps_of(chunk):
            if not (isinstance(step, int) and step == 0):
                first_arrival(step).wait_recv()
            share(step)

    def pass_on(chunk):
        for step in steps_of(chunk):
            for distance in range(1, highs):
                side_copy(step, distance).wait_recv()
                pair_copy(step, distance).start()

    def settle(chunk):
        for step in steps_of(chunk):
            for distance in range(highs):
                pair_copy(step, distance).wait_recv()

    def span(chunk):
        return pl.ds(chunk * group, group)

    tile = col_tile(ff_width)
    tiles = ff_width // tile
    out_tile = col_tile(width)

    def gate_up(chunk, first, last):
        rows = as_rows(arrived[span(chunk)])
        for index in range(first, last):
            columns = slice(index * tile, (index + 1) * tile)
            gate_val = jnp.dot(rows, gate[:, columns], preferred_element_type=jnp.float32)
            up_val = jnp.dot(rows, up[:, columns], preferred_element_type=jnp.float32)
            hidden[:, columns] = (jax.nn.silu(gate_val) * up_val).astype(jnp.bfloat16)

    def project(chunk):
        for index in range(width // out_tile):
            columns = slice(index * out_tile, (index + 1) * out_tile)
            block = jnp.dot(hidden[...], down[:, columns], preferred_element_type=jnp.float32)
            block = block.reshape(group, LANES, highs, cap, out_tile).astype(jnp.bfloat16)
            partial[span(chunk), :, :, :, columns] = block

    def back_pair_copy(chunk):
        return pltpu.make_async_remote_copy(
            src_ref=partial.at[span(chunk), other_low],
            dst_ref=pair_in.at[span(chunk)],
            send_sem=back_pair.at[0, chunk],
            recv_sem=back_pair.at[1, chunk],
            device_id=pair_id,
            device_id_type=MESH,
        )

    def back_side_copy(chunk, distance):
        return pltpu.make_async_remote_copy(
            src_ref=pair_sum.at[distance - 1, span(chunk)],
            dst_ref=side_in.at[distance - 1, span(chunk)],
            send_sem=back_side.at[0, chunk, distance - 1],
            recv_sem=back_side.at[1, chunk, distance - 1],
            device_id=side_id(distance),
            device_id_type=MESH,
        )

    def back_copy(step):
        peer = peer_of(step, me, sp_count)
        return pltpu.make_async_remote_copy(
            src_ref=served.at[step],
            dst_ref=returned.at[step_of(me, peer, sp_count)],
            send_sem=back_send.at[step],
            recv_sem=back_recv.at[step_of(me, peer, sp_count)],
            device_id=sp_id(peer),
            device_id_type=MESH,
        )

    def back_arrival(step):
        return pltpu.make_async_remote_copy(
            src_ref=served.at[step],
            dst_ref=returned.at[step],
            send_sem=back_send.at[step],
            recv_sem=back_recv.at[step],
            device_id=sp_id(peer_of(step, me, sp_count)),
            device_id_type=MESH,
        )

    def pair_add(chunk):
        back_pair_copy(chunk).wait_recv()
        for distance in range(1, highs):
            target = side_high(distance)
            for step in steps_of(chunk):
                total = partial[step, low, target].astype(jnp.float32)
                total = total + pair_in[step, target].astype(jnp.float32)
                pair_sum[distance - 1, step] = total.astype(jnp.bfloat16)
            back_side_copy(chunk, distance).start()

    def side_add(chunk):
        for distance in range(1, highs):
            back_side_copy(chunk, distance).wait_recv()
        for step in steps_of(chunk):
            total = partial[step, low, high].astype(jnp.float32)
            total = total + pair_in[step, high].astype(jnp.float32)
            for distance in range(1, highs):
                total = total + side_in[distance - 1, step].astype(jnp.float32)
            total = total.astype(jnp.bfloat16)

            def keep(step=step, total=total):
                returned[step] = total

            def give(step=step, total=total):
                served[step] = total
                back_copy(step).start()

            if isinstance(step, int):
                (keep if step == 0 else give)()
            else:
                pl.when(step == 0)(keep)
                pl.when(step > 0)(give)

    for step in range(1, sp_count):
        first_copy(step).start()
    arrived[0, :, :, :, columns_of(tp_me)] = send_ref[0]

    for chunk in range(min(SPREAD_AHEAD, chunks)):
        spread(chunk)
    for chunk in range(min(PASS_AHEAD, chunks)):
        pass_on(chunk)
    for copy in weight_copies:
        copy.wait()
    early = (tiles + 1) // 2

    def turn(chunk, carry):
        settle(chunk)
        gate_up(chunk, 0, early)

        @pl.when(chunk >= 1)
        def _():
            pair_add(chunk - 1)

        @pl.when(chunk + SPREAD_AHEAD < chunks)
        def _():
            spread(chunk + SPREAD_AHEAD)

        gate_up(chunk, early, tiles)

        @pl.when(chunk + PASS_AHEAD < chunks)
        def _():
            pass_on(chunk + PASS_AHEAD)

        @pl.when(chunk >= SIDE_LAG)
        def _():
            side_add(chunk - SIDE_LAG)

        project(chunk)
        back_pair_copy(chunk).start()
        return carry

    lax.fori_loop(0, chunks, turn, 0)
    pair_add(chunks - 1)
    for chunk in range(max(0, chunks - SIDE_LAG), chunks):
        side_add(chunk)

    for distance in range(1, tp_count):
        token_copy(distance).wait_recv()
    for step in range(1, sp_count):
        back_arrival(step).wait_recv()
    rows = as_rows(returned[...])
    route_weights = [as_column(weight_ref[pick : pick + 1, :]) for pick in range(top_count)]
    for piece in range(tp_count):
        columns = slice(piece * group_width, (piece + 1) * group_width)
        total = tokens[piece].astype(jnp.float32)
        for pick in range(top_count):
            picked = lax.dot_general(
                picked_at[tp_me, pick],
                rows[:, columns],
                (((0,), (0,)), ((), ())),
                preferred_element_type=jnp.float32,
            )
            total = total + route_weights[pick] * picked
        out_ref[:, columns] = total.astype(jnp.bfloat16)

    @pl.when(me + 1 < sp_count)
    def _():
        halo_copy.wait_send()

    for distance in range(1, tp_count):
        square_copy(distance).wait_send()
        square2_copy(distance).wait_send()
        route_copy(distance).wait_send()
        token_copy(distance).wait_send()

    def finish(step, carry):
        for distance in range(1, highs):
            side_copy(step, distance).wait_send()
        for distance in range(highs):
            pair_copy(step, distance).wait_send()
        return carry

    def finish_far(step, carry):
        first_copy(step).wait_send()
        back_copy(step).wait_send()
        return carry

    def finish_back(chunk, carry):
        back_pair_copy(chunk).wait_send()
        for distance in range(1, highs):
            back_side_copy(chunk, distance).wait_send()
        return carry

    lax.fori_loop(0, sp_count, finish, 0)
    lax.fori_loop(1, sp_count, finish_far, 0)
    lax.fori_loop(0, chunks, finish_back, 0)


def per_device(
    stream, mix_gain, pool_weight, pool_scale, ffn_gain, routes, route_weight, w_gate, w_up, w_down
):
    tok_rows, group_width = stream.shape
    tp_count = lax.axis_size("tp")
    sp_count = lax.axis_size("sp")
    width = group_width * tp_count
    tok_count, top_count = routes.shape
    cap = 2 * tok_count * top_count // sp_count
    halo_rows = 2 ** (pool_weight.shape[0] * tp_count)
    highs = tp_count // LANES
    chunks = chunk_count(sp_count)
    chunk_rows = sp_count // chunks * tp_count * cap
    ff_width = w_gate.shape[2]
    half = jnp.bfloat16
    vmem = pl.BlockSpec(memory_space=pltpu.VMEM)
    hbm = pl.BlockSpec(memory_space=pl.ANY)
    dma = pltpu.SemaphoreType.DMA
    rounds = max(1, sp_count // LANES - 1)
    return pl.pallas_call(
        functools.partial(expert_kernel, sp_count, tp_count, cap),
        out_shape=jax.ShapeDtypeStruct((tok_count, width), half),
        in_specs=[vmem] * 7 + [hbm] * 3,
        out_specs=vmem,
        scratch_shapes=[
            pltpu.VMEM((tp_count, 8, tok_rows), jnp.float32),
            pltpu.VMEM((tp_count, 8, tok_rows), jnp.float32),
            pltpu.VMEM((tp_count, top_count, tok_count), jnp.int32),
            pltpu.VMEM((halo_rows, group_width), half),
            pltpu.VMEM((halo_rows, group_width), half),
            pltpu.VMEM((tp_count, tok_count, group_width), half),
            pltpu.VMEM((tp_count, tok_count, group_width), half),
            pltpu.VMEM((tp_count, top_count, sp_count * cap, tok_count), half),
            pltpu.VMEM((sp_count, LANES, highs, cap, group_width), half),
            pltpu.VMEM(w_gate.shape[1:], half),
            pltpu.VMEM(w_up.shape[1:], half),
            pltpu.VMEM(w_down.shape[1:], half),
            pltpu.VMEM((sp_count, LANES, highs, cap, width), half),
            pltpu.VMEM((chunk_rows, ff_width), half),
            pltpu.VMEM((sp_count, LANES, highs, cap, width), half),
            pltpu.VMEM((sp_count, highs, cap, width), half),
            pltpu.VMEM((highs - 1, sp_count, cap, width), half),
            pltpu.VMEM((highs - 1, sp_count, cap, width), half),
            pltpu.VMEM((sp_count, cap, width), half),
            pltpu.VMEM((sp_count, cap, width), half),
            pltpu.SemaphoreType.REGULAR((rounds,)),
            dma((2, tp_count - 1)),
            dma((2, tp_count - 1)),
            dma((2, tp_count - 1)),
            dma((2,)),
            dma((2, tp_count - 1)),
            dma((3,)),
            dma((sp_count,)),
            dma((sp_count,)),
            dma((sp_count, highs - 1)),
            dma((sp_count, highs - 1)),
            dma((sp_count, highs)),
            dma((sp_count, highs)),
            dma((2, chunks)),
            dma((2, chunks, highs - 1)),
            dma((sp_count,)),
            dma((sp_count,)),
        ],
        compiler_params=pltpu.CompilerParams(
            collective_id=1, has_side_effects=True, vmem_limit_bytes=60 * 1024 * 1024
        ),
    )(
        stream,
        mix_gain,
        pool_weight,
        pool_scale,
        ffn_gain,
        routes.T,
        route_weight.T,
        w_gate,
        w_up,
        w_down,
    )


def solution(mesh):
    in_specs = (
        P("sp", "tp"),
        P("tp"),
        P("tp", None, None),
        P("tp"),
        P(),
        P(("sp", "tp"), None),
        P(("sp", "tp"), None),
        P("sp", None, "tp"),
        P("sp", None, "tp"),
        P("sp", "tp", None),
    )
    out_specs = P(("sp", "tp"), None)
    return jax.shard_map(
        per_device, mesh=mesh, in_specs=in_specs, out_specs=out_specs, check_vma=False
    )
```

time: 95.9 us -> 86.8 us (0.905)
  the two profiles are of different devices: /device:TPU:0 before, /device:TPU:10 now
where the time goes in v1:
time: 86.8 us; the launch traced here: 86.6 us
  Pallas kernels  85 us (98%)
  local copies, waits for them, and re-layouts  1.67 us (2%)
    pallas_call x1, Pallas kernels, per_device(): pl.pallas_call(functools.partial(expert_kernel, sp_count, tp_count, cap),...  85 us

profile of v1, /device:TPU:10, one launch (start us, length us, event | category | flops | bytes accessed | tf_op | source)
XLA Modules:
  0.0 86.6 jit_solution(11152958822972265778)
XLA Ops:
  0.0 85.0 %shard_map.100 = bf16[64,2048]{1,0:T(8,128)(2,1)} custom-call(bf16[256,512]{1,0:T(8,128)(2,1)} %stream_ref.1, bf16[512]{0:T(512)(128)(2,1)} %mix_ref.1, bf16[1,512,512]{2,1,0:T(8,128)(2,1)} %pool_ref.1, bf16[512]{0:T(512)(128)(2,1)} %scale_ref.1, bf16[2048]{0:T(1024)(128)(2,1)} %gain_ref.1, s32[2,64]{1,0:T(2,128)} %bitcast.2, f32[2,64]{1,0:T(2,128)} %bitcast.3, ...), custom_call_target="tpu_custom_call" | custom-call | tf_op jit(solution)/shard_map/pallas_call | solution.py:652
  85.0 1.7 %copy.12 = bf16[64,2048]{1,0:T(8,128)(2,1)} copy(bf16[64,2048]{1,0:T(8,128)(2,1)} %shard_map.100) | data formatting | bytes 524288

commit v2 on v1

--- a/solution.py
+++ b/solution.py
@@ -16,7 +16,10 @@
 CHUNKS = 8
 SPREAD_AHEAD = 3
 PASS_AHEAD = 1
-SIDE_LAG = 2
+SIDE_LAG = 3
+NEAR = 4
+ORDER = (0, 7, 6, 3, 5, 2, 4, 1)
+ISSUE = (1, 2, 4, 6, 3, 5, 7)
 
 
 def as_rows(block):
@@ -26,8 +29,24 @@
     return block.reshape(-1, width)
 
 
-def flip(code, sp_count):
-    return jnp.where(code == 0, 0, sp_count - code)
+def ranked(sp_count):
+    if sp_count == len(ORDER):
+        return ORDER
+    return tuple(range(sp_count))
+
+
+def looked_up(table, index):
+    found = jnp.zeros_like(index)
+    for key, value in enumerate(table):
+        found = jnp.where(index == key, value, found)
+    return found
+
+
+def code_of(step, sp_count):
+    table = ranked(sp_count)
+    if isinstance(step, int):
+        return jnp.int32(table[step])
+    return looked_up(table, step)
 
 
 def turned(me, code, sp_count):
@@ -38,11 +57,13 @@
 
 
 def step_of(peer, me, sp_count):
-    return flip(turned(me, peer ^ me, sp_count), sp_count)
+    table = ranked(sp_count)
+    places = [table.index(code) for code in range(sp_count)]
+    return looked_up(places, turned(me, peer ^ me, sp_count))
 
 
 def peer_of(step, me, sp_count):
-    return turned(me, flip(step, sp_count), sp_count) ^ me
+    return turned(me, code_of(step, sp_count), sp_count) ^ me
 
 
 def as_column(row):
@@ -88,9 +109,11 @@
     tail,
     halo,
     mixed,
+    mixed_far,
     tokens,
     picked_at,
     send_ref,
+    send_near,
     gate,
     up,
     down,
@@ -107,10 +130,12 @@
     square2_sem,
     route_sem,
     halo_sem,
+    raw_sem,
     token_sem,
     local_sem,
     first_send,
     first_recv,
+    near_send,
     side_send,
     side_recv,
     pair_send,
@@ -230,13 +255,28 @@
         device_id_type=MESH,
     )
 
+    def far_piece(distance):
+        return from_high(distance) * LANES + low
+
+    def raw_copy(distance):
+        return pltpu.make_async_remote_copy(
+            src_ref=mixed,
+            dst_ref=mixed_far.at[distance - 1],
+            send_sem=raw_sem.at[0, distance - 1],
+            recv_sem=raw_sem.at[1, distance - 1],
+            device_id=side_id(distance),
+            device_id_type=MESH,
+        )
+
     def token_copy(distance):
-        return pltpu.make_async_remote_copy(
-            src_ref=mixed.at[lax.rem(tp_me + distance, tp_count)],
-            dst_ref=tokens.at[tp_me],
-            send_sem=token_sem.at[0, distance - 1],
-            recv_sem=token_sem.at[1, distance - 1],
-            device_id=tp_id(distance),
+        block = high * LANES + other_low
+        source = mixed.at[block] if distance == 0 else mixed_far.at[distance - 1, block]
+        return pltpu.make_async_remote_copy(
+            src_ref=source,
+            dst_ref=tokens.at[far_piece(distance)],
+            send_sem=token_sem.at[0, distance],
+            recv_sem=token_sem.at[1, distance],
+            device_id=pair_id,
             device_id_type=MESH,
         )
 
@@ -317,8 +357,9 @@
     squares2[0] = jnp.broadcast_to(own_square, squares2.shape[1:])
     for distance in range(1, tp_count):
         square2_copy(distance).start()
-    for distance in range(1, tp_count):
-        token_copy(distance).start()
+    for distance in range(1, highs):
+        raw_copy(distance).start()
+    token_copy(0).start()
     tokens[tp_me] = mixed[tp_me]
 
     if pairs_count > 2:
@@ -343,11 +384,24 @@
             spot = jnp.sum(jnp.where(named[pick], rank, 0.0), axis=0, keepdims=True)
             spot = spot + start.astype(jnp.float32)
             picked_at[piece, pick] = jnp.where(slots == spot, 1.0, 0.0).astype(jnp.bfloat16)
-    gain = gain_ref[0:group_width]
-    for piece in range(1, tp_count):
-        columns = slice(piece * group_width, (piece + 1) * group_width)
-        gain = jnp.where(tp_me == piece, gain_ref[columns], gain)
-    gain = gain.astype(jnp.float32)[None, :]
+
+    def gain_of(own):
+        gain = gain_ref[0:group_width]
+        for piece in range(1, tp_count):
+            columns = slice(piece * group_width, (piece + 1) * group_width)
+            gain = jnp.where(own == piece, gain_ref[columns], gain)
+        return gain.astype(jnp.float32)[None, :]
+
+    table = ranked(sp_count)
+    near = [step for step in range(sp_count) if table[step] < NEAR]
+
+    def is_near(step):
+        if isinstance(step, int):
+            return step in near
+        found = step == near[0]
+        for index in near[1:]:
+            found = found | (step == index)
+        return found
 
     for distance in range(1, tp_count):
         square2_copy(distance).wait_recv()
@@ -355,7 +409,7 @@
     for distance in range(1, tp_count):
         square = square + squares2[distance, 0:1, :]
     ffn_scale = lax.rsqrt(as_column(square) / width + NORM_EPS)
-    normed2 = (after_f32 * ffn_scale * gain).astype(jnp.bfloat16)
+    normed2 = (after_f32 * ffn_scale * gain_of(tp_me)).astype(jnp.bfloat16)
     for index in range(2, pairs_count - 1):
         next_round(index)
     for piece in range(tp_count):
@@ -370,6 +424,41 @@
         rows = rows.reshape(sp_count, cap, group_width).astype(jnp.bfloat16)
         send_ref[:, piece % LANES, piece // LANES] = rows
 
+    def near_rows(piece):
+        spans = [slice(step * cap, (step + 1) * cap) for step in near]
+        parts = []
+        for part in spans:
+            rows = picked_at[piece, 0, part]
+            for pick in range(1, top_count):
+                rows = rows + picked_at[piece, pick, part]
+            parts.append(rows.astype(jnp.float32))
+        return jnp.concatenate(parts, axis=0).astype(jnp.bfloat16)
+
+    def fill_near(distance):
+        far_f32 = mixed_far[distance - 1].reshape(tok_rows, group_width).astype(jnp.float32)
+        far_gain = gain_of(far_piece(distance))
+        far_normed = (far_f32 * ffn_scale * far_gain).astype(jnp.bfloat16)
+        for piece in range(tp_count):
+            rows = jnp.dot(
+                near_rows(piece),
+                far_normed[piece * tok_count : (piece + 1) * tok_count],
+                preferred_element_type=jnp.float32,
+            )
+            rows = rows.reshape(len(near), cap, group_width).astype(jnp.bfloat16)
+            send_near[distance - 1, :, piece % LANES, piece // LANES] = rows
+
+    def near_copy(step, distance):
+        peer = peer_of(step, me, sp_count)
+        there = step_of(me, peer, sp_count)
+        return pltpu.make_async_remote_copy(
+            src_ref=send_near.at[distance - 1, near.index(step)],
+            dst_ref=arrived.at[there, :, :, :, columns_of(far_piece(distance))],
+            send_sem=near_send.at[near.index(step), distance - 1],
+            recv_sem=side_recv.at[there, distance - 1],
+            device_id=sp_id(peer),
+            device_id_type=MESH,
+        )
+
     def first_copy(step):
         peer = peer_of(step, me, sp_count)
         return pltpu.make_async_remote_copy(
@@ -417,9 +506,16 @@
     def steps_of(chunk):
         return [chunk * group + index for index in range(group)]
 
-    def share(step):
+    def to_sides(step):
         for distance in range(1, highs):
             side_copy(step, distance).start()
+
+    def share(step):
+        if isinstance(step, int):
+            if not is_near(step):
+                to_sides(step)
+        else:
+            pl.when(jnp.logical_not(is_near(step)))(lambda: to_sides(step))
         pair_copy(step, 0).start()
 
     def spread(chunk):
@@ -431,7 +527,8 @@
     def pass_on(chunk):
         for step in steps_of(chunk):
             for distance in range(1, highs):
-                side_copy(step, distance).wait_recv()
+                if not (isinstance(step, int) and step == 0):
+                    side_copy(step, distance).wait_recv()
                 pair_copy(step, distance).start()
 
     def settle(chunk):
@@ -535,13 +632,27 @@
                 pl.when(step == 0)(keep)
                 pl.when(step > 0)(give)
 
-    for step in range(1, sp_count):
+    issue = ISSUE if sp_count == len(ORDER) else tuple(range(1, sp_count))
+    for step in issue:
         first_copy(step).start()
     arrived[0, :, :, :, columns_of(tp_me)] = send_ref[0]
-
-    for chunk in range(min(SPREAD_AHEAD, chunks)):
+    if group == 1:
+        spread(0)
+    for distance in range(1, highs):
+        raw_copy(distance).wait_recv()
+        fill_near(distance)
+        for step in issue:
+            if step in near:
+                near_copy(step, distance).start()
+        arrived[0, :, :, :, columns_of(far_piece(distance))] = send_near[distance - 1, 0]
+        token_copy(distance).start()
+        tokens[far_piece(distance)] = mixed_far[distance - 1, tp_me]
+
+    if group == 1:
+        pass_on(0)
+    for chunk in range(0 if group > 1 else 1, min(SPREAD_AHEAD, chunks)):
         spread(chunk)
-    for chunk in range(min(PASS_AHEAD, chunks)):
+    for chunk in range(0 if group > 1 else 1, min(PASS_AHEAD, chunks)):
         pass_on(chunk)
     for copy in weight_copies:
         copy.wait()
@@ -578,7 +689,7 @@
     for chunk in range(max(0, chunks - SIDE_LAG), chunks):
         side_add(chunk)
 
-    for distance in range(1, tp_count):
+    for distance in range(highs):
         token_copy(distance).wait_recv()
     for step in range(1, sp_count):
         back_arrival(step).wait_recv()
@@ -605,11 +716,19 @@
         square_copy(distance).wait_send()
         square2_copy(distance).wait_send()
         route_copy(distance).wait_send()
+    for distance in range(highs):
         token_copy(distance).wait_send()
+    for distance in range(1, highs):
+        raw_copy(distance).wait_send()
+        for step in near[1:]:
+            near_copy(step, distance).wait_send()
 
     def finish(step, carry):
-        for distance in range(1, highs):
-            side_copy(step, distance).wait_send()
+        @pl.when(jnp.logical_not(is_near(step)))
+        def _():
+            for distance in range(1, highs):
+                side_copy(step, distance).wait_send()
+
         for distance in range(highs):
             pair_copy(step, distance).wait_send()
         return carry
@@ -661,9 +780,11 @@
             pltpu.VMEM((halo_rows, group_width), half),
             pltpu.VMEM((halo_rows, group_width), half),
             pltpu.VMEM((tp_count, tok_count, group_width), half),
+            pltpu.VMEM((highs - 1, tp_count, tok_count, group_width), half),
             pltpu.VMEM((tp_count, tok_count, group_width), half),
             pltpu.VMEM((tp_count, top_count, sp_count * cap, tok_count), half),
             pltpu.VMEM((sp_count, LANES, highs, cap, group_width), half),
+            pltpu.VMEM((highs - 1, min(NEAR, sp_count), LANES, highs, cap, group_width), half),
             pltpu.VMEM(w_gate.shape[1:], half),
             pltpu.VMEM(w_up.shape[1:], half),
             pltpu.VMEM(w_down.shape[1:], half),
@@ -680,10 +801,12 @@
             dma((2, tp_count - 1)),
             dma((2, tp_count - 1)),
             dma((2,)),
-            dma((2, tp_count - 1)),
+            dma((2, highs - 1)),
+            dma((2, highs)),
             dma((3,)),
             dma((sp_count,)),
             dma((sp_count,)),
+            dma((min(NEAR, sp_count), highs - 1)),
             dma((sp_count, highs - 1)),
             dma((sp_count, highs - 1)),
             dma((sp_count, highs)),

time: 86.8 us -> 75 us (0.86)
  Pallas kernels: 85 us -> 72.5 us
    pallas_call x1, Pallas kernels: 85 us -> 72.5 us  [per_device(): pl.pallas_call(functools.partial(expert_kernel, sp_count, tp_count, cap),...]
where the time goes in v2:
time: 75 us; the launch traced here: 74.1 us
  Pallas kernels  72.5 us (97%)
  local copies, waits for them, and re-layouts  1.67 us (2%)
    pallas_call x1, Pallas kernels, per_device(): pl.pallas_call(functools.partial(expert_kernel, sp_count, tp_count, cap),...  72.5 us
    unnamed x1, local copies, waits for them, and re-layouts  1.67 us

profile of v2, /device:TPU:10, one launch (start us, length us, event | category | flops | bytes accessed | tf_op | source)
XLA Modules:
  0.0 74.1 jit_solution(660333089389115220)
XLA Ops:
  0.0 72.5 %shard_map.100 = bf16[64,2048]{1,0:T(8,128)(2,1)} custom-call(bf16[256,512]{1,0:T(8,128)(2,1)} %stream_ref.1, bf16[512]{0:T(512)(128)(2,1)} %mix_ref.1, bf16[1,512,512]{2,1,0:T(8,128)(2,1)} %pool_ref.1, bf16[512]{0:T(512)(128)(2,1)} %scale_ref.1, bf16[2048]{0:T(1024)(128)(2,1)} %gain_ref.1, s32[2,64]{1,0:T(2,128)} %bitcast.2, f32[2,64]{1,0:T(2,128)} %bitcast.3, ...), custom_call_target="tpu_custom_call" | custom-call | tf_op jit(solution)/shard_map/pallas_call | solution.py:771
  72.5 1.7 %copy.12 = bf16[64,2048]{1,0:T(8,128)(2,1)} copy(bf16[64,2048]{1,0:T(8,128)(2,1)} %shard_map.100) | data formatting | bytes 524288

commit v3 on v2

--- a/solution.py
+++ b/solution.py
@@ -14,10 +14,12 @@
 COL_TILE = 256
 LANES = 2
 CHUNKS = 8
-SPREAD_AHEAD = 3
+SPREAD_AHEAD = 4
 PASS_AHEAD = 1
 SIDE_LAG = 3
+FIRST_SPREADS = 1
 NEAR = 4
+HALVES = 1
 ORDER = (0, 7, 6, 3, 5, 2, 4, 1)
 ISSUE = (1, 2, 4, 6, 3, 5, 7)
 
@@ -104,7 +106,6 @@
     down_hbm,
     out_ref,
     squares,
-    squares2,
     routes_all,
     tail,
     halo,
@@ -118,6 +119,7 @@
     up,
     down,
     arrived,
+    ready,
     hidden,
     partial,
     pair_in,
@@ -127,7 +129,6 @@
     returned,
     round_sem,
     square_sem,
-    square2_sem,
     route_sem,
     halo_sem,
     raw_sem,
@@ -226,16 +227,6 @@
             device_id_type=MESH,
         )
 
-    def square2_copy(distance):
-        return pltpu.make_async_remote_copy(
-            src_ref=squares2.at[0],
-            dst_ref=squares2.at[distance],
-            send_sem=square2_sem.at[0, distance - 1],
-            recv_sem=square2_sem.at[1, distance - 1],
-            device_id=tp_id(distance),
-            device_id_type=MESH,
-        )
-
     def route_copy(distance):
         return pltpu.make_async_remote_copy(
             src_ref=routes_ref,
@@ -334,36 +325,6 @@
         pl.semaphore_wait(round_sem.at[index], near_count)
         if index + 2 < pairs_count:
             tell_near(round_sem.at[index + 1])
-
-    if pairs_count > 1:
-        next_round(0)
-
-    @pl.when(me > 0)
-    def _():
-        halo_copy.wait_recv()
-
-    @pl.when(me == 0)
-    def _():
-        halo[...] = jnp.zeros_like(halo)
-
-    first_sum = window_sum[:halo_rows]
-    first_sum = first_sum + jnp.dot(halo_band, halo[...], preferred_element_type=jnp.float32)
-    first_mix = mix(
-        first_sum, window_count[:halo_rows], normed[:halo_rows], stream_f32[:halo_rows]
-    )
-    mixed[0, 0:halo_rows, :] = first_mix
-    after_f32 = mixed[...].reshape(tok_rows, group_width).astype(jnp.float32)
-    own_square = as_row(jnp.sum(after_f32 * after_f32, axis=1, keepdims=True))
-    squares2[0] = jnp.broadcast_to(own_square, squares2.shape[1:])
-    for distance in range(1, tp_count):
-        square2_copy(distance).start()
-    for distance in range(1, highs):
-        raw_copy(distance).start()
-    token_copy(0).start()
-    tokens[tp_me] = mixed[tp_me]
-
-    if pairs_count > 2:
-        next_round(1)
 
     experts = lax.broadcasted_iota(jnp.int32, (128, tok_count), 0)
     earlier = lax.broadcasted_iota(jnp.int32, (tok_count, tok_count), 0)
@@ -385,12 +346,30 @@
             spot = spot + start.astype(jnp.float32)
             picked_at[piece, pick] = jnp.where(slots == spot, 1.0, 0.0).astype(jnp.bfloat16)
 
-    def gain_of(own):
-        gain = gain_ref[0:group_width]
-        for piece in range(1, tp_count):
-            columns = slice(piece * group_width, (piece + 1) * group_width)
-            gain = jnp.where(own == piece, gain_ref[columns], gain)
-        return gain.astype(jnp.float32)[None, :]
+    if pairs_count > 1:
+        next_round(0)
+
+    @pl.when(me > 0)
+    def _():
+        halo_copy.wait_recv()
+
+    @pl.when(me == 0)
+    def _():
+        halo[...] = jnp.zeros_like(halo)
+
+    first_sum = window_sum[:halo_rows]
+    first_sum = first_sum + jnp.dot(halo_band, halo[...], preferred_element_type=jnp.float32)
+    first_mix = mix(
+        first_sum, window_count[:halo_rows], normed[:halo_rows], stream_f32[:halo_rows]
+    )
+    mixed[0, 0:halo_rows, :] = first_mix
+    for distance in range(1, highs):
+        raw_copy(distance).start()
+    token_copy(0).start()
+    tokens[tp_me] = mixed[tp_me]
+
+    if pairs_count > 2:
+        next_round(1)
 
     table = ranked(sp_count)
     near = [step for step in range(sp_count) if table[step] < NEAR]
@@ -403,13 +382,6 @@
             found = found | (step == index)
         return found
 
-    for distance in range(1, tp_count):
-        square2_copy(distance).wait_recv()
-    square = squares2[0, 0:1, :]
-    for distance in range(1, tp_count):
-        square = square + squares2[distance, 0:1, :]
-    ffn_scale = lax.rsqrt(as_column(square) / width + NORM_EPS)
-    normed2 = (after_f32 * ffn_scale * gain_of(tp_me)).astype(jnp.bfloat16)
     for index in range(2, pairs_count - 1):
         next_round(index)
     for piece in range(tp_count):
@@ -418,7 +390,7 @@
             dispatch = dispatch + picked_at[piece, pick]
         rows = jnp.dot(
             dispatch,
-            normed2[piece * tok_count : (piece + 1) * tok_count],
+            mixed[piece],
             preferred_element_type=jnp.float32,
         )
         rows = rows.reshape(sp_count, cap, group_width).astype(jnp.bfloat16)
@@ -435,13 +407,10 @@
         return jnp.concatenate(parts, axis=0).astype(jnp.bfloat16)
 
     def fill_near(distance):
-        far_f32 = mixed_far[distance - 1].reshape(tok_rows, group_width).astype(jnp.float32)
-        far_gain = gain_of(far_piece(distance))
-        far_normed = (far_f32 * ffn_scale * far_gain).astype(jnp.bfloat16)
         for piece in range(tp_count):
             rows = jnp.dot(
                 near_rows(piece),
-                far_normed[piece * tok_count : (piece + 1) * tok_count],
+                mixed_far[distance - 1, piece],
                 preferred_element_type=jnp.float32,
             )
             rows = rows.reshape(len(near), cap, group_width).astype(jnp.bfloat16)
@@ -541,90 +510,111 @@
 
     tile = col_tile(ff_width)
     tiles = ff_width // tile
-    out_tile = col_tile(width)
-
-    def gate_up(chunk, first, last):
-        rows = as_rows(arrived[span(chunk)])
+    half_width = width // HALVES
+    out_tile = col_tile(half_width)
+
+    def prepare(chunk):
+        square = jnp.zeros((chunk_rows, 1), jnp.float32)
+        for piece in range(tp_count):
+            columns = slice(piece * group_width, (piece + 1) * group_width)
+            rows = as_rows(arrived[span(chunk), :, :, :, columns]).astype(jnp.float32)
+            square = square + jnp.sum(rows * rows, axis=1, keepdims=True)
+        ffn_scale = lax.rsqrt(square / width + NORM_EPS)
+        for piece in range(tp_count):
+            columns = slice(piece * group_width, (piece + 1) * group_width)
+            rows = as_rows(arrived[span(chunk), :, :, :, columns]).astype(jnp.float32)
+            gain = gain_ref[columns].astype(jnp.float32)[None, :]
+            ready[:, columns] = (rows * ffn_scale * gain).astype(jnp.bfloat16)
+
+    def gate_up(first, last):
+        rows = ready[...]
         for index in range(first, last):
             columns = slice(index * tile, (index + 1) * tile)
             gate_val = jnp.dot(rows, gate[:, columns], preferred_element_type=jnp.float32)
             up_val = jnp.dot(rows, up[:, columns], preferred_element_type=jnp.float32)
             hidden[:, columns] = (jax.nn.silu(gate_val) * up_val).astype(jnp.bfloat16)
 
-    def project(chunk):
-        for index in range(width // out_tile):
+    def project(chunk, half):
+        per_half = half_width // out_tile
+        for index in range(half * per_half, (half + 1) * per_half):
             columns = slice(index * out_tile, (index + 1) * out_tile)
             block = jnp.dot(hidden[...], down[:, columns], preferred_element_type=jnp.float32)
             block = block.reshape(group, LANES, highs, cap, out_tile).astype(jnp.bfloat16)
             partial[span(chunk), :, :, :, columns] = block
 
-    def back_pair_copy(chunk):
-        return pltpu.make_async_remote_copy(
-            src_ref=partial.at[span(chunk), other_low],
-            dst_ref=pair_in.at[span(chunk)],
-            send_sem=back_pair.at[0, chunk],
-            recv_sem=back_pair.at[1, chunk],
+    def part_of(half):
+        return pl.ds(half * half_width, half_width)
+
+    def back_pair_copy(chunk, half):
+        return pltpu.make_async_remote_copy(
+            src_ref=partial.at[span(chunk), other_low, :, :, part_of(half)],
+            dst_ref=pair_in.at[span(chunk), :, :, part_of(half)],
+            send_sem=back_pair.at[0, chunk, half],
+            recv_sem=back_pair.at[1, chunk, half],
             device_id=pair_id,
             device_id_type=MESH,
         )
 
-    def back_side_copy(chunk, distance):
-        return pltpu.make_async_remote_copy(
-            src_ref=pair_sum.at[distance - 1, span(chunk)],
-            dst_ref=side_in.at[distance - 1, span(chunk)],
-            send_sem=back_side.at[0, chunk, distance - 1],
-            recv_sem=back_side.at[1, chunk, distance - 1],
+    def back_side_copy(chunk, half, distance):
+        return pltpu.make_async_remote_copy(
+            src_ref=pair_sum.at[distance - 1, span(chunk), :, part_of(half)],
+            dst_ref=side_in.at[distance - 1, span(chunk), :, part_of(half)],
+            send_sem=back_side.at[0, chunk, half, distance - 1],
+            recv_sem=back_side.at[1, chunk, half, distance - 1],
             device_id=side_id(distance),
             device_id_type=MESH,
         )
 
-    def back_copy(step):
+    def back_copy(step, half):
         peer = peer_of(step, me, sp_count)
-        return pltpu.make_async_remote_copy(
-            src_ref=served.at[step],
-            dst_ref=returned.at[step_of(me, peer, sp_count)],
-            send_sem=back_send.at[step],
-            recv_sem=back_recv.at[step_of(me, peer, sp_count)],
+        there = step_of(me, peer, sp_count)
+        return pltpu.make_async_remote_copy(
+            src_ref=served.at[step, :, part_of(half)],
+            dst_ref=returned.at[there, :, part_of(half)],
+            send_sem=back_send.at[step, half],
+            recv_sem=back_recv.at[there, half],
             device_id=sp_id(peer),
             device_id_type=MESH,
         )
 
-    def back_arrival(step):
-        return pltpu.make_async_remote_copy(
-            src_ref=served.at[step],
-            dst_ref=returned.at[step],
-            send_sem=back_send.at[step],
-            recv_sem=back_recv.at[step],
+    def back_arrival(step, half):
+        return pltpu.make_async_remote_copy(
+            src_ref=served.at[step, :, part_of(half)],
+            dst_ref=returned.at[step, :, part_of(half)],
+            send_sem=back_send.at[step, half],
+            recv_sem=back_recv.at[step, half],
             device_id=sp_id(peer_of(step, me, sp_count)),
             device_id_type=MESH,
         )
 
-    def pair_add(chunk):
-        back_pair_copy(chunk).wait_recv()
+    def pair_add(chunk, half):
+        columns = part_of(half)
+        back_pair_copy(chunk, half).wait_recv()
         for distance in range(1, highs):
             target = side_high(distance)
             for step in steps_of(chunk):
-                total = partial[step, low, target].astype(jnp.float32)
-                total = total + pair_in[step, target].astype(jnp.float32)
-                pair_sum[distance - 1, step] = total.astype(jnp.bfloat16)
-            back_side_copy(chunk, distance).start()
-
-    def side_add(chunk):
+                total = partial[step, low, target, :, columns].astype(jnp.float32)
+                total = total + pair_in[step, target, :, columns].astype(jnp.float32)
+                pair_sum[distance - 1, step, :, columns] = total.astype(jnp.bfloat16)
+            back_side_copy(chunk, half, distance).start()
+
+    def side_add(chunk, half):
+        columns = part_of(half)
         for distance in range(1, highs):
-            back_side_copy(chunk, distance).wait_recv()
+            back_side_copy(chunk, half, distance).wait_recv()
         for step in steps_of(chunk):
-            total = partial[step, low, high].astype(jnp.float32)
-            total = total + pair_in[step, high].astype(jnp.float32)
+            total = partial[step, low, high, :, columns].astype(jnp.float32)
+            total = total + pair_in[step, high, :, columns].astype(jnp.float32)
             for distance in range(1, highs):
-                total = total + side_in[distance - 1, step].astype(jnp.float32)
+                total = total + side_in[distance - 1, step, :, columns].astype(jnp.float32)
             total = total.astype(jnp.bfloat16)
 
             def keep(step=step, total=total):
-                returned[step] = total
+                returned[step, :, columns] = total
 
             def give(step=step, total=total):
-                served[step] = total
-                back_copy(step).start()
+                served[step, :, columns] = total
+                back_copy(step, half).start()
 
             if isinstance(step, int):
                 (keep if step == 0 else give)()
@@ -648,29 +638,47 @@
         token_copy(distance).start()
         tokens[far_piece(distance)] = mixed_far[distance - 1, tp_me]
 
-    if group == 1:
-        pass_on(0)
-    for chunk in range(0 if group > 1 else 1, min(SPREAD_AHEAD, chunks)):
-        spread(chunk)
-    for chunk in range(0 if group > 1 else 1, min(PASS_AHEAD, chunks)):
-        pass_on(chunk)
+    if group > 1:
+        spread(0)
+    pass_on(0)
     for copy in weight_copies:
         copy.wait()
     early = (tiles + 1) // 2
 
+    def finish_rows(chunk):
+        for half in range(HALVES):
+            project(chunk, half)
+            back_pair_copy(chunk, half).start()
+
+    settle(0)
+    prepare(0)
+    gate_up(0, tiles)
+    for chunk in range(1, min(1 + FIRST_SPREADS, chunks)):
+        spread(chunk)
+    finish_rows(0)
+    for chunk in range(1 + FIRST_SPREADS, min(SPREAD_AHEAD, chunks)):
+        spread(chunk)
+    for chunk in range(1, min(1 + PASS_AHEAD, chunks)):
+        pass_on(chunk)
+
     def turn(chunk, carry):
         settle(chunk)
-        gate_up(chunk, 0, early)
-
-        @pl.when(chunk >= 1)
-        def _():
-            pair_add(chunk - 1)
+        prepare(chunk)
+        gate_up(0, early)
+        for half in range(HALVES):
+            pair_add(chunk - 1, half)
+
+        if SPREAD_AHEAD < chunks:
+
+            @pl.when(chunk == 1)
+            def _():
+                spread(SPREAD_AHEAD)
 
         @pl.when(chunk + SPREAD_AHEAD < chunks)
         def _():
             spread(chunk + SPREAD_AHEAD)
 
-        gate_up(chunk, early, tiles)
+        gate_up(early, tiles)
 
         @pl.when(chunk + PASS_AHEAD < chunks)
         def _():
@@ -678,21 +686,28 @@
 
         @pl.when(chunk >= SIDE_LAG)
         def _():
-            side_add(chunk - SIDE_LAG)
-
-        project(chunk)
-        back_pair_copy(chunk).start()
+            for half in range(HALVES):
+                side_add(chunk - SIDE_LAG, half)
+
+        finish_rows(chunk)
         return carry
 
-    lax.fori_loop(0, chunks, turn, 0)
-    pair_add(chunks - 1)
-    for chunk in range(max(0, chunks - SIDE_LAG), chunks):
-        side_add(chunk)
+    lax.fori_loop(1, chunks, turn, 0)
+    last = chunks - 1
+    for chunk in range(max(0, chunks - SIDE_LAG), last - 1):
+        for half in range(HALVES):
+            side_add(chunk, half)
+    for half in range(HALVES):
+        pair_add(last, half)
+    for chunk in range(max(0, last - 1), chunks):
+        for half in range(HALVES):
+            side_add(chunk, half)
 
     for distance in range(highs):
         token_copy(distance).wait_recv()
     for step in range(1, sp_count):
-        back_arrival(step).wait_recv()
+        for half in range(HALVES):
+            back_arrival(step, half).wait_recv()
     rows = as_rows(returned[...])
     route_weights = [as_column(weight_ref[pick : pick + 1, :]) for pick in range(top_count)]
     for piece in range(tp_count):
@@ -714,7 +729,6 @@
 
     for distance in range(1, tp_count):
         square_copy(distance).wait_send()
-        square2_copy(distance).wait_send()
         route_copy(distance).wait_send()
     for distance in range(highs):
         token_copy(distance).wait_send()
@@ -735,13 +749,15 @@
 
     def finish_far(step, carry):
         first_copy(step).wait_send()
-        back_copy(step).wait_send()
+        for half in range(HALVES):
+            back_copy(step, half).wait_send()
         return carry
 
     def finish_back(chunk, carry):
-        back_pair_copy(chunk).wait_send()
-        for distance in range(1, highs):
-            back_side_copy(chunk, distance).wait_send()
+        for half in range(HALVES):
+            back_pair_copy(chunk, half).wait_send()
+            for distance in range(1, highs):
+                back_side_copy(chunk, half, distance).wait_send()
         return carry
 
     lax.fori_loop(0, sp_count, finish, 0)
@@ -775,7 +791,6 @@
         out_specs=vmem,
         scratch_shapes=[
             pltpu.VMEM((tp_count, 8, tok_rows), jnp.float32),
-            pltpu.VMEM((tp_count, 8, tok_rows), jnp.float32),
             pltpu.VMEM((tp_count, top_count, tok_count), jnp.int32),
             pltpu.VMEM((halo_rows, group_width), half),
             pltpu.VMEM((halo_rows, group_width), half),
@@ -789,6 +804,7 @@
             pltpu.VMEM(w_up.shape[1:], half),
             pltpu.VMEM(w_down.shape[1:], half),
             pltpu.VMEM((sp_count, LANES, highs, cap, width), half),
+            pltpu.VMEM((chunk_rows, width), half),
             pltpu.VMEM((chunk_rows, ff_width), half),
             pltpu.VMEM((sp_count, LANES, highs, cap, width), half),
             pltpu.VMEM((sp_count, highs, cap, width), half),
@@ -797,7 +813,6 @@
             pltpu.VMEM((sp_count, cap, width), half),
             pltpu.VMEM((sp_count, cap, width), half),
             pltpu.SemaphoreType.REGULAR((rounds,)),
-            dma((2, tp_count - 1)),
             dma((2, tp_count - 1)),
             dma((2, tp_count - 1)),
             dma((2,)),
@@ -811,10 +826,10 @@
             dma((sp_count, highs - 1)),
             dma((sp_count, highs)),
             dma((sp_count, highs)),
-            dma((2, chunks)),
-            dma((2, chunks, highs - 1)),
-            dma((sp_count,)),
-            dma((sp_count,)),
+            dma((2, chunks, HALVES)),
+            dma((2, chunks, HALVES, highs - 1)),
+            dma((sp_count, HALVES)),
+            dma((sp_count, HALVES)),
         ],
         compiler_params=pltpu.CompilerParams(
             collective_id=1, has_side_effects=True, vmem_limit_bytes=60 * 1024 * 1024

time: 75 us -> 73.3 us (0.977)
  Pallas kernels: 72.5 us -> 71.5 us
    pallas_call x1, Pallas kernels: 72.5 us -> 71.5 us  [per_device(): pl.pallas_call(functools.partial(expert_kernel, sp_count, tp_count, cap),...]
where the time goes in v3:
time: 73.3 us; the launch traced here: 73.2 us
  Pallas kernels  71.5 us (98%)
  local copies, waits for them, and re-layouts  1.67 us (2%)
    pallas_call x1, Pallas kernels, per_device(): pl.pallas_call(functools.partial(expert_kernel, sp_count, tp_count, cap),...  71.5 us
    unnamed x1, local copies, waits for them, and re-layouts  1.67 us

profile of v3, /device:TPU:10, one launch (start us, length us, event | category | flops | bytes accessed | tf_op | source)
XLA Modules:
  0.0 73.2 jit_solution(9324016520498463036)
XLA Ops:
  0.0 71.5 %shard_map.100 = bf16[64,2048]{1,0:T(8,128)(2,1)} custom-call(bf16[256,512]{1,0:T(8,128)(2,1)} %stream_ref.1, bf16[512]{0:T(512)(128)(2,1)} %mix_ref.1, bf16[1,512,512]{2,1,0:T(8,128)(2,1)} %pool_ref.1, bf16[512]{0:T(512)(128)(2,1)} %scale_ref.1, bf16[2048]{0:T(1024)(128)(2,1)} %gain_ref.1, s32[2,64]{1,0:T(2,128)} %bitcast.2, f32[2,64]{1,0:T(2,128)} %bitcast.3, ...), custom_call_target="tpu_custom_call" | custom-call | tf_op jit(solution)/shard_map/pallas_call | solution.py:787
  71.5 1.7 %copy.12 = bf16[64,2048]{1,0:T(8,128)(2,1)} copy(bf16[64,2048]{1,0:T(8,128)(2,1)} %shard_map.100) | data formatting | bytes 524288

commit v4 on v3

--- a/solution.py
+++ b/solution.py
@@ -127,6 +127,7 @@
     side_in,
     served,
     returned,
+    summed,
     round_sem,
     square_sem,
     route_sem,
@@ -705,23 +706,33 @@
 
     for distance in range(highs):
         token_copy(distance).wait_recv()
-    for step in range(1, sp_count):
-        for half in range(HALVES):
-            back_arrival(step, half).wait_recv()
-    rows = as_rows(returned[...])
     route_weights = [as_column(weight_ref[pick : pick + 1, :]) for pick in range(top_count)]
-    for piece in range(tp_count):
-        columns = slice(piece * group_width, (piece + 1) * group_width)
-        total = tokens[piece].astype(jnp.float32)
-        for pick in range(top_count):
-            picked = lax.dot_general(
-                picked_at[tp_me, pick],
-                rows[:, columns],
-                (((0,), (0,)), ((), ())),
-                preferred_element_type=jnp.float32,
-            )
-            total = total + route_weights[pick] * picked
-        out_ref[:, columns] = total.astype(jnp.bfloat16)
+
+    def gather(first, last):
+        for step in range(max(1, first), last):
+            for half in range(HALVES):
+                back_arrival(step, half).wait_recv()
+        rows = as_rows(returned[first:last])
+        for piece in range(tp_count):
+            columns = slice(piece * group_width, (piece + 1) * group_width)
+            total = tokens[piece].astype(jnp.float32) if first == 0 else summed[:, columns]
+            for pick in range(top_count):
+                picked = lax.dot_general(
+                    picked_at[tp_me, pick, first * cap : last * cap],
+                    rows[:, columns],
+                    (((0,), (0,)), ((), ())),
+                    preferred_element_type=jnp.float32,
+                )
+                total = total + route_weights[pick] * picked
+            if last == sp_count:
+                out_ref[:, columns] = total.astype(jnp.bfloat16)
+            else:
+                summed[:, columns] = total
+
+    middle = sp_count * 5 // 8
+    if middle:
+        gather(0, middle)
+    gather(middle, sp_count)
 
     @pl.when(me + 1 < sp_count)
     def _():
@@ -812,6 +823,7 @@
             pltpu.VMEM((highs - 1, sp_count, cap, width), half),
             pltpu.VMEM((sp_count, cap, width), half),
             pltpu.VMEM((sp_count, cap, width), half),
+            pltpu.VMEM((tok_count, width), jnp.float32),
             pltpu.SemaphoreType.REGULAR((rounds,)),
             dma((2, tp_count - 1)),
             dma((2, tp_count - 1)),

time: 73.3 us -> 73.1 us (level)
  no operation moved by 1% of the time
where the time goes in v4:
time: 73.1 us; the launch traced here: 73 us
  Pallas kernels  71.3 us (98%)
  local copies, waits for them, and re-layouts  1.67 us (2%)
    pallas_call x1, Pallas kernels, per_device(): pl.pallas_call(functools.partial(expert_kernel, sp_count, tp_count, cap),...  71.3 us
    unnamed x1, local copies, waits for them, and re-layouts  1.67 us

profile of v4, /device:TPU:10, one launch (start us, length us, event | category | flops | bytes accessed | tf_op | source)
XLA Modules:
  0.0 73.0 jit_solution(7661209346339442041)
XLA Ops:
  0.0 71.3 %shard_map.100 = bf16[64,2048]{1,0:T(8,128)(2,1)} custom-call(bf16[256,512]{1,0:T(8,128)(2,1)} %stream_ref.1, bf16[512]{0:T(512)(128)(2,1)} %mix_ref.1, bf16[1,512,512]{2,1,0:T(8,128)(2,1)} %pool_ref.1, bf16[512]{0:T(512)(128)(2,1)} %scale_ref.1, bf16[2048]{0:T(1024)(128)(2,1)} %gain_ref.1, s32[2,64]{1,0:T(2,128)} %bitcast.2, f32[2,64]{1,0:T(2,128)} %bitcast.3, ...), custom_call_target="tpu_custom_call" | custom-call | tf_op jit(solution)/shard_map/pallas_call | solution.py:798
  71.3 1.7 %copy.12 = bf16[64,2048]{1,0:T(8,128)(2,1)} copy(bf16[64,2048]{1,0:T(8,128)(2,1)} %shard_map.100) | data formatting | bytes 524288
